TPU v7x, 32 devices: a whole 2x2x4 slice. The times are simulated.
32 devices in a mesh: kv: 8 (over z, y), tp: 4 (over x, core).
Axes of the slice: x: 2, y: 2, z: 4, core: 2. Of those that a mesh axis runs over, the one named last changes fastest.
Arguments:
- piece_tokens: bfloat16 [1024, 4096], P('kv'), may hold values from -6 to 6
- decode_tokens: bfloat16 [8, 4096], P('kv'), may hold values from -6 to 6
- norm_gain: bfloat16 [4096], replicated, may hold values from 0.099609375 to 1.8984375
- w_query: bfloat16 [4096, 2048], P(None, 'tp'), may hold values from -0.09375 to 0.09375
- w_key: bfloat16 [4096, 2048], P(None, 'tp'), may hold values from -0.09375 to 0.09375
- w_value: bfloat16 [4096, 2048], P(None, 'tp'), may hold values from -0.09375 to 0.09375
- score_offset: float32 [16], replicated, may hold values from -14 to -3
- context_length: int32 [1], replicated, may hold values from 4096 to 8192
- prompt_keys: bfloat16 [8192, 2048], P('kv', 'tp'), may hold values from -16 to 16, as said below
- prompt_values: bfloat16 [8192, 2048], P('kv', 'tp'), may hold values from -6 to 6
- decode_keys: bfloat16 [8, 1024, 2048], P('kv', None, 'tp'), may hold values from -6 to 6
- decode_values: bfloat16 [8, 1024, 2048], P('kv', None, 'tp'), may hold values from -6 to 6
- decoding_cache_length: int32 [8], P('kv'), may hold values from 1 to 1024, as said below
- out_gain: bfloat16 [2048], replicated, may hold values from 0.099609375 to 1.8984375
- w_out: bfloat16 [2048, 4096], P(None, 'tp'), may hold values from -0.125 to 0.125
Outputs:
- prompt_piece_output: bfloat16 [1024, 4096], P('kv', 'tp')
- decode_out: bfloat16 [8, 4096], P('kv', 'tp')
- piece_keys: bfloat16 [1024, 2048], P('kv', 'tp')
- piece_values: bfloat16 [1024, 2048], P('kv', 'tp')
- decode_new_keys: bfloat16 [8, 2048], P('kv', 'tp')
- decode_new_values: bfloat16 [8, 2048], P('kv', 'tp')
Inputs may be any that keep to these rules, and one draw needn't show every extreme that they name: `prompt_keys`: the largest scale of a block of 1024 positions is up to four times the smallest. `decoding_cache_length`: some sequence has exactly 1024 valid positions.
All inputs are finite; a program needn't handle non-finite values.
Results may differ from a plain program's by a relative error of at most 0.008.
The roundings to bfloat16 on the way count: a program that leaves them out, or rounds other values in their place, can miss the bound.
Values may be sent and summed in bfloat16 or wider, within the bound.
A program may use at most 128 MiB of HBM per device.

v0:
```python
import math

import jax
import jax.numpy as jnp
from jax import lax
from jax.sharding import PartitionSpec as P

HEAD = 128


EPS = 1e-06


def rms_scaled(rows, gain):
    values = rows.astype(jnp.float32)
    inverse = lax.rsqrt(jnp.mean(values * values, axis=-1, keepdims=True) + EPS)
    return values * inverse * gain.astype(jnp.float32)


def block_terms(scores, visible):
    keep = jnp.where(visible, jax.nn.log_sigmoid(-scores), 0.0)
    after = lax.cumsum(keep, axis=scores.ndim - 1, reverse=True) - keep
    weight = jnp.where(visible, jnp.exp(jax.nn.log_sigmoid(scores) + after), 0.0)
    return (weight.astype(jnp.bfloat16), jnp.sum(keep, axis=-1))


def shard_terms(
    query_rows, places, cache_keys, cache_values, new_k, new_v, offset, valid_mask, key_start
):
    score_scale = query_rows.shape[-1] ** (-0.5)
    cache_scores = jnp.einsum(
        "qhd,khd->hqk", query_rows, cache_keys, preferred_element_type=jnp.float32
    )
    cache_scores = cache_scores * score_scale + offset[:, None, None]
    cached_weight_rows, cache_total = block_terms(cache_scores, valid_mask[None, None, :])
    cached_output = jnp.einsum(
        "hqk,khd->qhd", cached_weight_rows, cache_values, preferred_element_type=jnp.float32
    )
    key_places = key_start + jnp.arange(new_k.shape[0], dtype=jnp.int32)
    piece_scores = jnp.einsum("qhd,khd->hqk", query_rows, new_k, preferred_element_type=jnp.float32)
    piece_scores = piece_scores * score_scale + offset[:, None, None]
    seen = key_places[None, None, :] < places[None, :, None]
    prompt_piece_weight, piece_total = block_terms(piece_scores, seen)
    prompt_piece_output = jnp.einsum(
        "hqk,khd->qhd", prompt_piece_weight, new_v, preferred_element_type=jnp.float32
    )
    return (cached_output, prompt_piece_output, cache_total.T, piece_total.T)


def attend_queries(local_queries, cache_keys, cache_values, new_k, new_v, offset, valid_mask):
    row_count = local_queries.shape[0]
    gathered = lax.all_gather(local_queries, "kv", axis=0, tiled=True)
    total_rows = gathered.shape[0]
    kv_count = lax.axis_size("kv")
    kv_index = lax.axis_index("kv")
    local_heads = offset.shape[0]
    head_size = gathered.shape[1] // local_heads
    places = jnp.arange(total_rows, dtype=jnp.int32)
    block_rows = math.gcd(total_rows, 512)
    query_blocks = gathered.reshape(total_rows // block_rows, block_rows, local_heads, head_size)
    place_blocks = places.reshape(total_rows // block_rows, block_rows)
    key_start = kv_index * row_count

    def block_fn(inputs_pair):
        return shard_terms(
            inputs_pair[0],
            inputs_pair[1],
            cache_keys,
            cache_values,
            new_k,
            new_v,
            offset,
            valid_mask,
            key_start,
        )

    cached_output, prompt_piece_output, cache_total, piece_total = lax.map(
        block_fn, (query_blocks, place_blocks)
    )
    cached_output = cached_output.reshape(total_rows, local_heads, head_size)
    prompt_piece_output = prompt_piece_output.reshape(total_rows, local_heads, head_size)
    cache_total = cache_total.reshape(total_rows, local_heads)
    piece_total = piece_total.reshape(total_rows, local_heads)
    every_cache, every_piece = (
        lax.all_gather(cache_total[None], "kv", axis=0, tiled=True),
        lax.all_gather(piece_total[None], "kv", axis=0, tiled=True),
    )
    is_later = (jnp.arange(kv_count, dtype=jnp.int32) > kv_index)[:, None, None]
    later_cache = jnp.sum(jnp.where(is_later, every_cache, 0.0), axis=0)
    later_piece = jnp.sum(jnp.where(is_later, every_piece, 0.0), axis=0)
    piece_sum = jnp.sum(every_piece, axis=0)
    weighted = cached_output * jnp.exp(later_cache + piece_sum)[:, :, None]
    weighted = weighted + prompt_piece_output * jnp.exp(later_piece)[:, :, None]
    weighted = weighted.reshape(total_rows, local_heads * head_size)
    own_rows = lax.psum_scatter(weighted, "kv", scatter_dimension=0, tiled=True)
    return own_rows.astype(jnp.bfloat16)


def body(
    piece_tokens,
    decode_tokens,
    norm_gain,
    w_query,
    w_key,
    w_value,
    score_offset,
    context_length,
    prompt_keys,
    prompt_values,
    decode_keys,
    decode_values,
    decoding_cache_length,
    out_gain,
    w_out,
):
    head_size = HEAD
    local_width = w_query.shape[1]
    local_heads = local_width // head_size
    offset = lax.dynamic_slice_in_dim(score_offset, lax.axis_index("tp") * local_heads, local_heads)
    piece_rows = piece_tokens.shape[0]
    all_rows = jnp.concatenate([piece_tokens, decode_tokens], axis=0)
    normed_in = rms_scaled(all_rows, norm_gain).astype(jnp.bfloat16)
    queries = jnp.dot(normed_in, w_query, preferred_element_type=jnp.float32).astype(jnp.bfloat16)
    new_keys = jnp.dot(normed_in, w_key, preferred_element_type=jnp.float32).astype(jnp.bfloat16)
    new_values = jnp.dot(normed_in, w_value, preferred_element_type=jnp.float32).astype(
        jnp.bfloat16
    )
    cache_rows = prompt_keys.shape[0]
    cache_keys = prompt_keys.reshape(cache_rows, local_heads, head_size)
    cache_values = prompt_values.reshape(cache_rows, local_heads, head_size)
    new_k = new_keys[:piece_rows].reshape(piece_rows, local_heads, head_size)
    new_v = new_values[:piece_rows].reshape(piece_rows, local_heads, head_size)
    piece_queries = queries[:piece_rows]
    cache_places = lax.axis_index("kv") * cache_rows + jnp.arange(cache_rows, dtype=jnp.int32)
    valid_mask = cache_places < context_length[0]
    piece_attention = attend_queries(
        piece_queries, cache_keys, cache_values, new_k, new_v, offset, valid_mask
    )
    seq_count = decode_tokens.shape[0]
    slot_count = decode_keys.shape[1]
    decode_queries = queries[piece_rows:].reshape(seq_count, local_heads, head_size)
    seq_keys = decode_keys.reshape(seq_count, slot_count, local_heads, head_size)
    seq_values = decode_values.reshape(seq_count, slot_count, local_heads, head_size)
    decode_scores = jnp.einsum(
        "shd,skhd->shk", decode_queries, seq_keys, preferred_element_type=jnp.float32
    )
    decode_scores = decode_scores * head_size ** (-0.5) + offset[None, :, None]
    seen = (
        jnp.arange(slot_count, dtype=jnp.int32)[None, None, :]
        < decoding_cache_length[:, None, None]
    )
    decode_weight, unused = block_terms(decode_scores, seen)
    decode_attention = jnp.einsum(
        "shk,skhd->shd", decode_weight, seq_values, preferred_element_type=jnp.float32
    )
    decode_attention = decode_attention.astype(jnp.bfloat16).reshape(seq_count, local_width)
    attention = jnp.concatenate([piece_attention, decode_attention], axis=0)
    gathered = lax.all_gather(attention, "tp", axis=1, tiled=True)
    normed_out = rms_scaled(gathered, out_gain).astype(jnp.bfloat16)
    outputs = jnp.dot(normed_out, w_out, preferred_element_type=jnp.float32).astype(jnp.bfloat16)
    return (
        outputs[:piece_rows],
        outputs[piece_rows:],
        new_keys[:piece_rows],
        new_values[:piece_rows],
        new_keys[piece_rows:],
        new_values[piece_rows:],
    )


def solution(mesh):
    in_specs = (
        P("kv", None),
        P("kv", None),
        P(),
        P(None, "tp"),
        P(None, "tp"),
        P(None, "tp"),
        P(),
        P(),
        P("kv", "tp"),
        P("kv", "tp"),
        P("kv", None, "tp"),
        P("kv", None, "tp"),
        P("kv"),
        P(),
        P(None, "tp"),
    )
    out_specs = (
        P("kv", "tp"),
        P("kv", "tp"),
        P("kv", "tp"),
        P("kv", "tp"),
        P("kv", "tp"),
        P("kv", "tp"),
    )
    return jax.shard_map(body, mesh=mesh, in_specs=in_specs, out_specs=out_specs, check_vma=False)
```

profile of v0, /device:TPU:13, one launch (start us, length us, event | category | flops | bytes accessed | tf_op | source)
XLA Modules:
  0.0 488.7 jit_solution(3321729040373105010)
XLA Ops:
  9.6 3.3 convolution_convert_fusion.3
  20.1 3.0 convolution_convert_fusion.1
  24.7 28.3 %all-gather.2.cloned.1.call-done = bf16[1024,512]{1,0:T(8,128)(2,1)} async-done(((bf16[128,512]{1,0:T(8,128)(2,1)}), bf16[1024,512]{1,0:T(8,128)(2,1)}) %all-gather.2.cloned.1.call-update) | async-done | bytes 1048592 | tf_op jit(solution)/shard_map/all_gather | solution.py:52
  55.2 275.1 %while.17 = (s32[]{:T(128)}, f32[2,512,4,128]{3,2,1,0:T(4,128)}, f32[2,512,4,128]{3,2,1,0:T(4,128)}, f32[2,512,4]{1,2,0:T(4,128)}, f32[2,512,4]{1,2,0:T(4,128)},...) while((s32[]{:T(128)}, f32[2,512,4,128]{3,2,1,0:T(4,128)}, ...), condition=%wide.region_7.8_spmd.clone, body=%wide.region_1.7_spmd.clone.sunk | while | flops 1593700480 | bytes 322308800 | solution.py:77
  60.5 7.0 %fusion.91 = (f32[4,512]{1,0:T(4,128)S(1)}, f32[4,512,1024]{2,1,0:T(8,128)S(1)}) fusion(f32[4]{0:T(128)} %get-tuple-element.367, f32[4,512,1024]{2,1,0:T(8,128)S(1)} %get-tuple-element.317, u8[512,1024]{1,0:T(8,128)(4,1)S(1)} %get-tuple-element.318, pred[1024]{0:T(1024)(128)(4,1)S(1)} %add_compare_fusion.2), kind=kLoop, calls=%fused_computation.103.clone.1 | loop fusion | flops 29358080 | bytes 17310736 | tf_op jit(solution)/shard_map/while/body/eval_jaxpr/reduce_sum | solution.py:24
  67.6 5.7 %copy.133 = f32[256,8,8,128]{3,2,1,0:T(8,128)} copy(f32[256,8,8,128]{3,1,2,0:T(8,128)S(1)} %bitcast.159) | data formatting | bytes 16777216 | tf_op jit(solution)/shard_map/while
  73.3 10.7 %copy.134 = f32[4,512,8,128]{1,2,3,0:T(8,128)} copy(f32[4,512,8,128]{3,2,1,0:T(8,128)} %bitcast.160) | data formatting | bytes 16777216 | tf_op jit(solution)/shard_map/reshape
  84.1 30.0 %fusion.92 = f32[4,512,8,128]{1,2,3,0:T(8,128)S(1)} fusion(f32[4,512,8,128]{1,2,3,0:T(8,128)} %copy.134), kind=kOutput, calls=%fused_computation.104.clone.1 | output fusion | flops 266338304 | bytes 16777216 | tf_op jit(solution)/shard_map/reduce-window
  114.0 3.2 copy-done
  117.4 7.7 %broadcast_add_fusion.2 = f32[4,512,8,128]{1,2,3,0:T(8,128)} fusion(f32[4,512,8,128]{1,2,3,0:T(8,128)} %copy-done, f32[4,512,8]{1,2,0:T(8,128)S(1)} %slice.73), kind=kLoop, calls=%fused_computation.11.clone.1 | loop fusion | flops 2097152 | bytes 16842752 | tf_op jit(solution)/shard_map/reduce_window_sum | solution.py:22
  125.1 10.4 %copy.135 = f32[4,512,8,128]{3,2,1,0:T(8,128)} copy(f32[4,512,8,128]{1,2,3,0:T(8,128)} %broadcast_add_fusion.2) | data formatting | bytes 16777216 | tf_op jit(solution)/shard_map/reduce_window_sum | solution.py:22
  135.5 9.4 %reduce_window_sum.54 = f32[4,512,1024]{2,1,0:T(8,128)} reshape(f32[4,512,8,128]{3,2,1,0:T(8,128)} %copy.135) | data formatting | bytes 16777216 | tf_op jit(solution)/shard_map/reduce_window_sum | solution.py:22
  144.8 11.8 %fusion.93 = f32[1,512,4,128]{3,1,2,0:T(8,128)S(1)} fusion(bf16[1024,4,128]{2,0,1:T(8,128)(2,1)S(1)} %copy-done.16, f32[4,512,1024]{2,1,0:T(8,128)} %reduce_window_sum.54, f32[4,512,1024]{2,1,0:T(8,128)} %copy-done.1, f32[4,512,1024]{2,1,0:T(8,128)} %copy-done.2, f32[4]{0:T(128)} %get-tuple-element.367, pred[1024]{0:T(1024)(128)(4,1)S(1)} %add_compare_fusion.2), kind=kOutput, calls=%fused_computation.18.clone.1 | convolution fusion | flops 566231040 | bytes 27264016 | tf_op jit(solution)/shard_map/while/body/eval_jaxpr/hqk,khd->qhd/dot_general | solution.py:36
  159.2 27.6 %reduce_window_sum.53 = f32[4,512,128]{1,2,0:T(8,128)S(1)} reduce-window(f32[4,512,128]{1,2,0:T(8,128)S(1)} %get-tuple-element.316, f32[]{:T(128)} %constant.60.clone.1..sunk), window={size=1x1x128 pad=0_0x0_0x0_127}, to_apply=%region_4.4 | reduce-window | flops 33292288 | bytes 2097156 | tf_op jit(solution)/shard_map/while/body/eval_jaxpr/reduce_window_sum | solution.py:22
  186.9 3.1 convolution_bitcast_fusion.2
  200.2 7.0 %fusion.91 = (f32[4,512]{1,0:T(4,128)S(1)}, f32[4,512,1024]{2,1,0:T(8,128)S(1)}) fusion(f32[4]{0:T(128)} %get-tuple-element.367, f32[4,512,1024]{2,1,0:T(8,128)S(1)} %get-tuple-element.317, u8[512,1024]{1,0:T(8,128)(4,1)S(1)} %get-tuple-element.318, pred[1024]{0:T(1024)(128)(4,1)S(1)} %add_compare_fusion.2), kind=kLoop, calls=%fused_computation.103.clone.1 | loop fusion | flops 29358080 | bytes 17310736 | tf_op jit(solution)/shard_map/while/body/eval_jaxpr/reduce_sum | solution.py:24
  207.2 5.7 %copy.133 = f32[256,8,8,128]{3,2,1,0:T(8,128)} copy(f32[256,8,8,128]{3,1,2,0:T(8,128)S(1)} %bitcast.159) | data formatting | bytes 16777216 | tf_op jit(solution)/shard_map/while
  212.9 10.6 %copy.134 = f32[4,512,8,128]{1,2,3,0:T(8,128)} copy(f32[4,512,8,128]{3,2,1,0:T(8,128)} %bitcast.160) | data formatting | bytes 16777216 | tf_op jit(solution)/shard_map/reshape
  223.6 21.1 %fusion.92 = f32[4,512,8,128]{1,2,3,0:T(8,128)S(1)} fusion(f32[4,512,8,128]{1,2,3,0:T(8,128)} %copy.134), kind=kOutput, calls=%fused_computation.104.clone.1 | output fusion | flops 266338304 | bytes 16777216 | tf_op jit(solution)/shard_map/reduce-window
  244.7 3.2 copy-done
  248.0 7.7 %broadcast_add_fusion.2 = f32[4,512,8,128]{1,2,3,0:T(8,128)} fusion(f32[4,512,8,128]{1,2,3,0:T(8,128)} %copy-done, f32[4,512,8]{1,2,0:T(8,128)S(1)} %slice.73), kind=kLoop, calls=%fused_computation.11.clone.1 | loop fusion | flops 2097152 | bytes 16842752 | tf_op jit(solution)/shard_map/reduce_window_sum | solution.py:22
  255.7 10.4 %copy.135 = f32[4,512,8,128]{3,2,1,0:T(8,128)} copy(f32[4,512,8,128]{1,2,3,0:T(8,128)} %broadcast_add_fusion.2) | data formatting | bytes 16777216 | tf_op jit(solution)/shard_map/reduce_window_sum | solution.py:22
  266.1 9.4 %reduce_window_sum.54 = f32[4,512,1024]{2,1,0:T(8,128)} reshape(f32[4,512,8,128]{3,2,1,0:T(8,128)} %copy.135) | data formatting | bytes 16777216 | tf_op jit(solution)/shard_map/reduce_window_sum | solution.py:22
  275.5 11.8 %fusion.93 = f32[1,512,4,128]{3,1,2,0:T(8,128)S(1)} fusion(bf16[1024,4,128]{2,0,1:T(8,128)(2,1)S(1)} %copy-done.16, f32[4,512,1024]{2,1,0:T(8,128)} %reduce_window_sum.54, f32[4,512,1024]{2,1,0:T(8,128)} %copy-done.1, f32[4,512,1024]{2,1,0:T(8,128)} %copy-done.2, f32[4]{0:T(128)} %get-tuple-element.367, pred[1024]{0:T(1024)(128)(4,1)S(1)} %add_compare_fusion.2), kind=kOutput, calls=%fused_computation.18.clone.1 | convolution fusion | flops 566231040 | bytes 27264016 | tf_op jit(solution)/shard_map/while/body/eval_jaxpr/hqk,khd->qhd/dot_general | solution.py:36
  289.9 27.4 %reduce_window_sum.53 = f32[4,512,128]{1,2,0:T(8,128)S(1)} reduce-window(f32[4,512,128]{1,2,0:T(8,128)S(1)} %get-tuple-element.316, f32[]{:T(128)} %constant.60.clone.1..sunk), window={size=1x1x128 pad=0_0x0_0x0_127}, to_apply=%region_4.4 | reduce-window | flops 33292288 | bytes 2097156 | tf_op jit(solution)/shard_map/while/body/eval_jaxpr/reduce_window_sum | solution.py:22
  317.3 3.1 convolution_bitcast_fusion.2
  330.3 20.6 %all_gather.13 = f32[8,1024,4]{1,2,0:T(4,128)S(1)} all-gather(f32[1,1024,4]{1,2,0:T(4,128)} %bitcast.169), channel_id=1, replica_groups=mesh['kv'=8,'tp'=4] {'kv'}, dimensions={0}, use_global_device_ids=true | all-gather | bytes 147456 | tf_op jit(solution)/shard_map/all_gather | solution.py:85
  350.8 24.4 %all_gather.14 = f32[8,1024,4]{1,2,0:T(4,128)S(1)} all-gather(f32[1,1024,4]{1,2,0:T(4,128)} %bitcast.170), channel_id=1, replica_groups=mesh['kv'=8,'tp'=4] {'kv'}, dimensions={0}, use_global_device_ids=true | all-gather | bytes 147456 | tf_op jit(solution)/shard_map/all_gather | solution.py:86
  386.8 5.0 %reduce-window.16 = f32[1,4,8,128]{3,2,1,0:T(8,128)S(1)} reduce-window(f32[1,4,8,128]{3,2,1,0:T(8,128)S(1)} %copy.122, f32[]{:T(128)} %constant.60.clone.1), window={size=1x1x1x128 pad=0_0x0_0x0_0x0_127}, to_apply=%region_12.13 | reduce-window | flops 520192 | bytes 32772 | tf_op jit(solution)/shard_map/reduce-window.2
  393.5 73.0 %reduce-scatter.2.cloned.1.call-done = f32[128,512]{1,0:T(8,128)} async-done(((f32[1024,512]{1,0:T(8,128)}), f32[128,512]{1,0:T(8,128)}) %reduce-scatter.2.cloned.1.call-update) | async-done | bytes 262160 | tf_op jit(solution)/shard_map/reduce_scatter | solution.py:95
  467.5 9.3 %all_gather.15 = bf16[129,2048]{1,0:T(8,128)(2,1)S(1)} all-gather(bf16[129,512]{1,0:T(8,128)(2,1)S(1)} %pad_maximum_fusion.1), channel_id=1, replica_groups=mesh['kv'=8,'tp'=4] {'tp'}, dimensions={1}, use_global_device_ids=true | all-gather | bytes 660480 | tf_op jit(solution)/shard_map/all_gather | solution.py:158
  477.0 3.1 convolution_convert_fusion
  (169 shorter events, 53.5 us)
Async XLA Ops:
  7.2 45.9 %all-gather.2.cloned.1.call-start = ((), (), s32[]{:S(2)}) async-start(), calls=%async_computation.1 | async-start | bytes 1179648 | tf_op jit(solution)/shard_map/all_gather | solution.py:52
  7.9 6.4 %copy-start.11 = (bf16[1024,512]{1,0:T(8,128)(2,1)S(1)}, bf16[1024,512]{1,0:T(8,128)(2,1)}, u32[]{:S(2)}) copy-start(bf16[1024,512]{1,0:T(8,128)(2,1)} %param.25) | copy-start | bytes 3145732
  14.2 452.3 %reduce-scatter.2.cloned.1.call-start = ((), (), s32[]{:S(2)}) async-start(), calls=%async_computation.2 | async-start | bytes 2359296 | tf_op jit(solution)/shard_map/reduce_scatter | solution.py:95
  14.4 4.1 copy-start.29
  14.4 5.8 %copy-start.10 = (bf16[128,4096]{1,0:T(8,128)(2,1)S(1)}, bf16[128,4096]{1,0:T(8,128)(2,1)}, u32[]{:S(2)}) copy-start(bf16[128,4096]{1,0:T(8,128)(2,1)} %param.17) | copy-start | bytes 3145732
  14.4 5.7 %copy-start.22 = (bf16[1,4096]{1,0:T(2,128)(2,1)S(1)}, bf16[1,4096]{1,0:T(2,128)(2,1)}, u32[]{:S(2)}) copy-start(bf16[1,4096]{1,0:T(2,128)(2,1)} %param.18) | copy-start | bytes 24580
  18.4 4.7 copy-start.28
  55.4 4.5 copy-start.14
  59.9 7.7 %copy-start.2 = (f32[4,512,1024]{2,1,0:T(8,128)}, f32[4,512,1024]{2,1,0:T(8,128)S(1)}, u32[]{:S(2)}) copy-start(f32[4,512,1024]{2,1,0:T(8,128)S(1)} %get-tuple-element.317) | copy-start | bytes 25165828 | tf_op jit(solution)/shard_map/while
  67.6 5.7 %copy-start.1 = (f32[4,512,1024]{2,1,0:T(8,128)}, f32[4,512,1024]{2,1,0:T(8,128)S(1)}, u32[]{:S(2)}) copy-start(f32[4,512,1024]{2,1,0:T(8,128)S(1)} %get-tuple-element.319) | copy-start | bytes 25165828 | tf_op jit(solution)/shard_map/while
  114.0 3.2 copy-start
  135.5 9.4 %copy-start.16 = (bf16[1024,4,128]{2,0,1:T(8,128)(2,1)S(1)}, bf16[1024,4,128]{2,0,1:T(8,128)(2,1)}, u32[]{:S(2)}) copy-start(bf16[1024,4,128]{2,0,1:T(8,128)(2,1)} %get-tuple-element.368) | copy-start | bytes 3145732 | tf_op jit(solution)/shard_map/while
  186.9 3.1 copy-start.4
  186.9 3.1 copy-start.7
  186.9 7.3 %copy-start.23 = (f32[2,512,4]{1,2,0:T(4,128)S(1)}, f32[2,512,4]{1,2,0:T(4,128)}, u32[]{:S(2)}) copy-start(f32[2,512,4]{1,2,0:T(4,128)} %get-tuple-element.346) | copy-start | bytes 49156 | tf_op jit(solution)/shard_map/while
  186.9 7.3 %copy-start.25 = (f32[2,512,4]{1,2,0:T(4,128)S(1)}, f32[2,512,4]{1,2,0:T(4,128)}, u32[]{:S(2)}) copy-start(f32[2,512,4]{1,2,0:T(4,128)} %get-tuple-element.347) | copy-start | bytes 49156 | tf_op jit(solution)/shard_map/while
  190.0 4.8 copy-start.15
  195.0 4.5 copy-start.14
  199.5 7.7 %copy-start.2 = (f32[4,512,1024]{2,1,0:T(8,128)}, f32[4,512,1024]{2,1,0:T(8,128)S(1)}, u32[]{:S(2)}) copy-start(f32[4,512,1024]{2,1,0:T(8,128)S(1)} %get-tuple-element.317) | copy-start | bytes 25165828 | tf_op jit(solution)/shard_map/while
  207.2 5.7 %copy-start.1 = (f32[4,512,1024]{2,1,0:T(8,128)}, f32[4,512,1024]{2,1,0:T(8,128)S(1)}, u32[]{:S(2)}) copy-start(f32[4,512,1024]{2,1,0:T(8,128)S(1)} %get-tuple-element.319) | copy-start | bytes 25165828 | tf_op jit(solution)/shard_map/while
  244.7 3.2 copy-start
  266.1 9.4 %copy-start.16 = (bf16[1024,4,128]{2,0,1:T(8,128)(2,1)S(1)}, bf16[1024,4,128]{2,0,1:T(8,128)(2,1)}, u32[]{:S(2)}) copy-start(bf16[1024,4,128]{2,0,1:T(8,128)(2,1)} %get-tuple-element.368) | copy-start | bytes 3145732 | tf_op jit(solution)/shard_map/while
  317.3 3.1 copy-start.4
  317.3 3.1 copy-start.7
  317.3 7.3 %copy-start.23 = (f32[2,512,4]{1,2,0:T(4,128)S(1)}, f32[2,512,4]{1,2,0:T(4,128)}, u32[]{:S(2)}) copy-start(f32[2,512,4]{1,2,0:T(4,128)} %get-tuple-element.346) | copy-start | bytes 49156 | tf_op jit(solution)/shard_map/while
  317.3 7.3 %copy-start.25 = (f32[2,512,4]{1,2,0:T(4,128)S(1)}, f32[2,512,4]{1,2,0:T(4,128)}, u32[]{:S(2)}) copy-start(f32[2,512,4]{1,2,0:T(4,128)} %get-tuple-element.347) | copy-start | bytes 49156 | tf_op jit(solution)/shard_map/while
  320.4 4.8 copy-start.15
  330.3 48.6 %copy-start.6 = (f32[2,512,4,128]{3,2,1,0:T(4,128)S(1)}, f32[2,512,4,128]{3,2,1,0:T(4,128)}, u32[]{:S(2)}) copy-start(f32[2,512,4,128]{3,2,1,0:T(4,128)} %get-tuple-element.81) | copy-start | bytes 6291460
  379.0 3.1 copy-start.18
  379.0 5.0 %copy-start.12 = (bf16[1,1024,512]{2,1,0:T(8,128)(2,1)S(1)}, bf16[1,1024,512]{2,1,0:T(8,128)(2,1)}, u32[]{:S(2)}) copy-start(bf16[1,1024,512]{2,1,0:T(8,128)(2,1)} %param.27) | copy-start | bytes 3145732
  381.4 10.6 %copy-start.13 = (bf16[1,1024,512]{2,1,0:T(8,128)(2,1)S(1)}, bf16[1,1024,512]{2,1,0:T(8,128)(2,1)}, u32[]{:S(2)}) copy-start(bf16[1,1024,512]{2,1,0:T(8,128)(2,1)} %param.28) | copy-start | bytes 3145732
  381.4 12.1 %copy-start.27 = (bf16[2048]{0:T(1024)(128)(2,1)S(1)}, bf16[2048]{0:T(1024)(128)(2,1)}, u32[]{:S(2)}) copy-start(bf16[2048]{0:T(1024)(128)(2,1)} %param.30) | copy-start | bytes 12292
  (15 other events, 18.2 us)
Sparse Core Ops, SparseCore 0:
  14.4 38.6 all-gather.1
  381.5 84.9 reduce-scatter.1
where the time goes:
time: 495 us; the launch traced here: 489 us
  other arithmetic  153 us (31%)
  local copies, waits for them, and re-layouts  110 us (22%)
  waiting for transfers between devices  101 us (20%)
  blocking collectives  54.2 us (11%)
  matrix products  48.8 us (10%)
  between operations  15.6 us (3%)
  loops' own time  5.89 us (1%)
    reduce_scatter x1, waiting for transfers between devices, attend_queries(): own_rows = lax.psum_scatter(weighted, 'kv', scatter_dimension=0, tiled=True)  73 us
    another operation x4, other arithmetic, block_terms(): after = lax.cumsum(keep, axis=scores.ndim - 1, reverse=True) - keep  70.4 us
    another operation x10, other arithmetic  56.4 us
    another operation x4, local copies, waits for them, and re-layouts, block_terms(): after = lax.cumsum(keep, axis=scores.ndim - 1, reverse=True) - keep  39.5 us
    all_gather x1, waiting for transfers between devices, attend_queries(): gathered = lax.all_gather(local_queries, 'kv', axis=0, tiled=True)  28.3 us
    while x62, local copies, waits for them, and re-layouts  24.4 us
    all_gather x1, blocking collectives, attend_queries(): lax.all_gather(piece_total[None], 'kv', axis=0, tiled=True)  24.4 us
    dot_general x2, matrix products, shard_terms(): jnp.einsum('hqk,khd->qhd', cached_weight_rows, cache_values, preferred_el...  23.5 us
  transfers between devices with their start and end apart: 2, of which 2 were waited for; matrix products, arithmetic and copies ran while one was open for 4% of the time, Pallas kernels for 0%

commit v1 on v0

v1 whole, which is shorter than its diff:
```python
import functools

import jax
import jax.numpy as jnp
from jax import lax
from jax.experimental import pallas as pl
from jax.experimental.pallas import tpu as pltpu
from jax.sharding import PartitionSpec as P

HEAD = 128
EPS = 1e-06
HIDDEN = -1e30
MESH = pl.DeviceIdType.MESH


def rms_scaled(rows, gain):
    values = rows.astype(jnp.float32)
    inverse = lax.rsqrt(jnp.mean(values * values, axis=-1, keepdims=True) + EPS)
    return values * inverse * gain.astype(jnp.float32)


def suffix_matrix(size):
    row = lax.broadcasted_iota(jnp.int32, (size, size), 0)
    column = lax.broadcasted_iota(jnp.int32, (size, size), 1)
    return jnp.where(row >= column, 1.0, 0.0).astype(jnp.bfloat16)


def dot_t(a, b):
    return lax.dot_general(a, b, (((1,), (1,)), ((), ())), preferred_element_type=jnp.float32)


def dot(a, b):
    return jnp.dot(a, b, preferred_element_type=jnp.float32)


def suffix_keep(z, suffix):
    keep = -(jnp.maximum(z, 0.0) + jnp.log(1.0 + jnp.exp(-jnp.abs(z))))
    high = keep.astype(jnp.bfloat16)
    low = (keep - high.astype(jnp.float32)).astype(jnp.bfloat16)
    return dot(high, suffix) + dot(low, suffix)


def cached_terms(query, key_of, value_of, bias_of, total_keys, chunk, suffix, scale):
    later = None
    out = None
    for start in reversed(range(0, total_keys, chunk)):
        z = dot_t(query, key_of(start)) * scale + bias_of(start)
        inner = suffix_keep(z, suffix)
        exponent = z + inner if later is None else z + inner + later
        weight = jnp.exp(exponent).astype(jnp.bfloat16)
        part = dot(weight, value_of(start))
        out = part if out is None else out + part
        later = inner[:, 0:1] if later is None else later + inner[:, 0:1]
    return out, later


def attention_kernel(
    n, tp, heads, q_ref, k_ref, v_ref, dq_ref, ck_ref, cv_ref, cbias_ref, off_ref, dk_ref, dv_ref,
    dbias_ref, gain_ref, out_ref, qg, kg, vg, osend, orecv, tsend, trecv, acc, later_s, att, attg,
    q_ss, q_rs, k_ss, k_rs, v_ss, v_rs, o_ss, o_rs, t_ss, t_rs, a_ss, a_rs,
):
    me = lax.axis_index("kv")
    mine = lax.axis_index("tp")
    rows = q_ref.shape[0]
    cache_rows = ck_ref.shape[0]
    seqs, slots = dk_ref.shape[0], dk_ref.shape[1]
    scale = HEAD ** (-0.5)
    chunk = 256 if cache_rows % 256 == 0 else 128

    barrier = pltpu.get_barrier_semaphore()
    for s in range(1, n):
        pl.semaphore_signal(barrier, inc=1, device_id={"kv": lax.rem(me + s, n)}, device_id_type=MESH)
    for s in range(1, tp):
        pl.semaphore_signal(barrier, inc=1, device_id={"tp": lax.rem(mine + s, tp)}, device_id_type=MESH)
    pl.semaphore_wait(barrier, n - 1 + tp - 1)

    def remote(src, dst, ss, rs, peer, axis="kv"):
        return pltpu.make_async_remote_copy(
            src_ref=src, dst_ref=dst, send_sem=ss, recv_sem=rs,
            device_id={axis: peer}, device_id_type=MESH,
        )

    def send_all(src, dst, ss, rs):
        for s in range(1, n):
            peer = lax.rem(me + n - s, n)
            remote(src, dst.at[me], ss.at[s], rs.at[me], peer).start()

    send_all(q_ref, qg, q_ss, q_rs)
    send_all(k_ref, kg, k_ss, k_rs)
    send_all(v_ref, vg, v_ss, v_rs)
    qg[me] = q_ref[...]
    kg[me] = k_ref[...]
    vg[me] = v_ref[...]

    wide = suffix_matrix(chunk)
    width = heads * HEAD
    hrow = lax.broadcasted_iota(jnp.int32, (8, width), 0)
    hcol = lax.broadcasted_iota(jnp.int32, (8, width), 1) // HEAD
    own_head = hrow == hcol
    att[pl.ds(rows, 16), :] = jnp.zeros((16, width), att.dtype)
    dec_rows = jnp.zeros((16, width), jnp.float32)
    for b in range(seqs):
        query = jnp.where(own_head, dq_ref[b : b + 1, :].astype(jnp.float32), 0.0).astype(jnp.bfloat16)
        out, unused = cached_terms(
            query,
            lambda start: dk_ref[b, pl.ds(start, chunk), :],
            lambda start: dv_ref[b, pl.ds(start, chunk), :],
            lambda start: dbias_ref[b, :, pl.ds(start, chunk)],
            slots, chunk, wide, scale,
        )
        row = jnp.sum(jnp.where(own_head, out, 0.0), axis=0, keepdims=True)
        place = lax.broadcasted_iota(jnp.int32, (16, width), 0)
        dec_rows = jnp.where(place == b, row, dec_rows)
    att[pl.ds(rows, 16), :] = dec_rows.astype(att.dtype)

    lane = lax.broadcasted_iota(jnp.int32, (rows, 128), 1)

    def block(s, carry):
        owner = lax.rem(me + s, n)

        @pl.when(s > 0)
        def _():
            remote(q_ref, qg.at[owner], q_ss.at[s], q_rs.at[owner], owner).wait_recv()

        totals = jnp.zeros((rows, 128), jnp.float32)
        for h in range(heads):
            cols = pl.ds(h * HEAD, HEAD)
            out, total = cached_terms(
                qg[owner, :, cols],
                lambda start: ck_ref[pl.ds(start, chunk), cols],
                lambda start: cv_ref[pl.ds(start, chunk), cols],
                lambda start: cbias_ref[h : h + 1, pl.ds(start, chunk)],
                cache_rows, chunk, wide, scale,
            )
            osend[owner, :, cols] = out.astype(jnp.bfloat16)
            totals = jnp.where(lane == h, total, totals)
        tsend[owner] = jnp.transpose(totals)[0:8, :]

        @pl.when(s > 0)
        def _():
            place = pl.ds(pl.multiple_of(me * 8, 8), 8)
            remote(tsend.at[owner], trecv.at[place], t_ss.at[s], t_rs.at[me], owner).start()
            remote(osend.at[owner], orecv.at[me], o_ss.at[s], o_rs.at[me], owner).start()

        return carry

    lax.fori_loop(0, n, block, 0)
    orecv[me] = osend[me]
    trecv[pl.ds(pl.multiple_of(me * 8, 8), 8), :] = tsend[me]

    for s in range(1, n):
        peer = lax.rem(me + s, n)
        remote(k_ref, kg.at[peer], k_ss.at[s], k_rs.at[peer], peer).wait()
        remote(v_ref, vg.at[peer], v_ss.at[s], v_rs.at[peer], peer).wait()
        remote(q_ref, qg.at[peer], q_ss.at[s], q_rs.at[peer], peer).wait_send()

    narrow = suffix_matrix(rows)
    qrow = lax.broadcasted_iota(jnp.int32, (rows, rows), 0)
    kcol = lax.broadcasted_iota(jnp.int32, (rows, rows), 1)
    acc[...] = jnp.zeros_like(acc)

    def piece(step, later):
        j = n - 1 - step
        seen = (j * rows + kcol) < (me * rows + qrow)
        nexts = []
        for h in range(heads):
            cols = pl.ds(h * HEAD, HEAD)
            z = dot_t(q_ref[:, cols], kg[j, :, cols]) * scale + off_ref[h : h + 1, 0:1]
            z = jnp.where(seen, z, HIDDEN)
            inner = suffix_keep(z, narrow)
            weight = jnp.exp(z + inner).astype(jnp.bfloat16)
            acc[:, cols] += dot(weight, vg[j, :, cols]) * jnp.exp(later[h])
            nexts.append(later[h] + inner[:, 0:1])
        return tuple(nexts)

    piece_total = lax.fori_loop(
        0, n, piece, tuple(jnp.zeros((rows, 1), jnp.float32) for _ in range(heads))
    )

    for s in range(1, n):
        peer = lax.rem(me + s, n)
        place = pl.ds(pl.multiple_of(peer * 8, 8), 8)
        remote(tsend.at[peer], trecv.at[place], t_ss.at[s], t_rs.at[peer], peer).wait()
        remote(osend.at[peer], orecv.at[peer], o_ss.at[s], o_rs.at[peer], peer).wait()

    run = jnp.zeros((8, 128), jnp.float32)
    later_s[...] = jnp.zeros_like(later_s)
    for c in reversed(range(n)):
        later_s[c * 8 : c * 8 + 8, :] = run
        run = run + trecv[c * 8 : c * 8 + 8, :]
    factors = [
        jnp.exp(jnp.transpose(later_s[g * 128 : g * 128 + 128, :]))
        for g in range(later_s.shape[0] // 128)
    ]
    for h in range(heads):
        cols = pl.ds(h * HEAD, HEAD)
        mixed = jnp.zeros((rows, HEAD), jnp.float32)
        for c in range(n):
            group, spot = divmod(c * 8 + h, 128)
            mixed += orecv[c, :, cols].astype(jnp.float32) * factors[group][:, spot : spot + 1]
        mixed = mixed * jnp.exp(piece_total[h]) + acc[:, cols]
        att[pl.ds(0, rows), cols] = mixed.astype(att.dtype)

    for s in range(1, tp):
        peer = lax.rem(mine + s, tp)
        remote(att, attg.at[mine], a_ss.at[s], a_rs.at[mine], peer, "tp").start()
    attg[mine] = att[...]
    for s in range(1, tp):
        peer = lax.rem(mine + s, tp)
        remote(att, attg.at[peer], a_ss.at[s], a_rs.at[peer], peer, "tp").wait()
    square = jnp.zeros((att.shape[0], 1), jnp.float32)
    for t in range(tp):
        values = attg[t].astype(jnp.float32)
        square += jnp.sum(values * values, axis=-1, keepdims=True)
    inverse = lax.rsqrt(square / (tp * width) + EPS)
    for t in range(tp):
        cols = pl.ds(t * width, width)
        gain = gain_ref[0:1, cols].astype(jnp.float32)
        out_ref[:, cols] = (attg[t].astype(jnp.float32) * inverse * gain).astype(out_ref.dtype)


def body(
    piece_tokens, decode_tokens, norm_gain, w_query, w_key, w_value, score_offset, context_length,
    prompt_keys, prompt_values, decode_keys, decode_values, decoding_cache_length, out_gain, w_out,
):
    n, tp = lax.axis_size("kv"), lax.axis_size("tp")
    width = w_query.shape[1]
    heads = width // HEAD
    offset = lax.dynamic_slice_in_dim(score_offset, lax.axis_index("tp") * heads, heads)
    offset = jnp.pad(offset, (0, 8 - heads))
    rows = piece_tokens.shape[0]
    all_rows = jnp.concatenate([piece_tokens, decode_tokens], axis=0)
    normed_in = rms_scaled(all_rows, norm_gain).astype(jnp.bfloat16)
    queries = jnp.dot(normed_in, w_query, preferred_element_type=jnp.float32).astype(jnp.bfloat16)
    new_keys = jnp.dot(normed_in, w_key, preferred_element_type=jnp.float32).astype(jnp.bfloat16)
    new_values = jnp.dot(normed_in, w_value, preferred_element_type=jnp.float32).astype(
        jnp.bfloat16
    )
    cache_rows = prompt_keys.shape[0]
    seqs, slots = decode_keys.shape[:2]
    places = lax.axis_index("kv") * cache_rows + jnp.arange(cache_rows, dtype=jnp.int32)
    cache_bias = jnp.where(places[None, :] < context_length[0], offset[:, None], HIDDEN)
    spots = jnp.arange(slots, dtype=jnp.int32)[None, None, :]
    decode_bias = jnp.where(
        spots < decoding_cache_length[:, None, None], offset[None, :, None], HIDDEN
    )
    wide_offset = jnp.broadcast_to(offset[:, None], (8, 128))
    trows = -(-n * 8 // 128) * 128
    vmem = pl.BlockSpec(memory_space=pltpu.VMEM)
    dma = pltpu.SemaphoreType.DMA
    block = pltpu.VMEM((n, rows, width), jnp.bfloat16)
    normed_out = pl.pallas_call(
        functools.partial(attention_kernel, n, tp, heads),
        out_shape=jax.ShapeDtypeStruct((rows + 16, tp * width), jnp.bfloat16),
        in_specs=[vmem] * 12,
        out_specs=vmem,
        scratch_shapes=[
            block, block, block, block, block,
            pltpu.VMEM((n, 8, 128), jnp.float32),
            pltpu.VMEM((trows, 128), jnp.float32),
            pltpu.VMEM((rows, width), jnp.float32),
            pltpu.VMEM((trows, 128), jnp.float32),
            pltpu.VMEM((rows + 16, width), jnp.bfloat16),
            pltpu.VMEM((tp, rows + 16, width), jnp.bfloat16),
        ] + [dma((n,)) for _ in range(10)] + [dma((tp,)), dma((tp,))],
        compiler_params=pltpu.CompilerParams(
            collective_id=0, has_side_effects=True, vmem_limit_bytes=56 * 1024 * 1024
        ),
        name="attend",
    )(
        queries[:rows], new_keys[:rows], new_values[:rows], queries[rows:], prompt_keys,
        prompt_values, cache_bias, wide_offset, decode_keys, decode_values, decode_bias,
        out_gain[None, :],
    )
    outputs = jnp.dot(normed_out, w_out, preferred_element_type=jnp.float32).astype(jnp.bfloat16)
    return (
        outputs[:rows],
        outputs[rows : rows + seqs],
        new_keys[:rows],
        new_values[:rows],
        new_keys[rows:],
        new_values[rows:],
    )


def solution(mesh):
    in_specs = (
        P("kv", None),
        P("kv", None),
        P(),
        P(None, "tp"),
        P(None, "tp"),
        P(None, "tp"),
        P(),
        P(),
        P("kv", "tp"),
        P("kv", "tp"),
        P("kv", None, "tp"),
        P("kv", None, "tp"),
        P("kv"),
        P(),
        P(None, "tp"),
    )
    out_specs = (
        P("kv", "tp"),
        P("kv", "tp"),
        P("kv", "tp"),
        P("kv", "tp"),
        P("kv", "tp"),
        P("kv", "tp"),
    )
    return jax.shard_map(body, mesh=mesh, in_specs=in_specs, out_specs=out_specs, check_vma=False)
```

time: 495 us -> 129 us (0.26); the launches traced: 489 us -> 129 us
  other arithmetic: 153 us -> 3.63 us
  Pallas kernels: 0 us -> 108 us
  local copies, waits for them, and re-layouts: 110 us -> 7.92 us
  waiting for transfers between devices: 101 us -> 0 us
  blocking collectives: 54.2 us -> 0 us
  matrix products: 48.8 us -> 6.87 us
  between operations: 15.6 us -> 2 us
  loops' own time: 5.89 us -> 0 us
    another operation x14 -> x0, other arithmetic: 127 us -> none  [the longest x4 70.4 us: block_terms(): after = lax.cumsum(keep, axis=scores.ndim - 1, reverse=True) - keep]
    pallas_call x0 -> x1, Pallas kernels: none -> 108 us  [body(): pl.pallas_call(functools.partial(attention_kernel, n, tp, heads), out_sha...]
    reduce_scatter x1 -> x0, waiting for transfers between devices: 73 us -> none  [attend_queries(): own_rows = lax.psum_scatter(weighted, 'kv', scatter_dimension=0, tiled=True)]
    all_gather x3 -> x0, blocking collectives: 54.2 us -> none  [the longest x1 24.4 us: attend_queries(): lax.all_gather(piece_total[None], 'kv', axis=0, tiled=True)]
    another operation x12 -> x0, local copies, waits for them, and re-layouts: 40.5 us -> none  [the longest x4 39.5 us: block_terms(): after = lax.cumsum(keep, axis=scores.ndim - 1, reverse=True) - keep]
    dot_general x10 -> x0, matrix products: 38.6 us -> none  [the longest x2 23.5 us: shard_terms(): jnp.einsum('hqk,khd->qhd', cached_weight_rows, cache_values, preferred_el...]
    all_gather x1 -> x0, waiting for transfers between devices: 28.3 us -> none  [attend_queries(): gathered = lax.all_gather(local_queries, 'kv', axis=0, tiled=True)]
    while x62 -> x0, local copies, waits for them, and re-layouts: 24.4 us -> none
  transfers between devices with their start and end apart: 2 -> 0, of which waited for: 2 -> 0; matrix products, arithmetic and copies ran while one was open for 4% -> 0% of each run, Pallas kernels for 0% -> 0%
where the time goes in v1:
time: 129 us
  Pallas kernels  108 us (84%)
  local copies, waits for them, and re-layouts  7.92 us (6%)
  matrix products  6.87 us (5%)
  other arithmetic  3.63 us (3%)
  between operations  2 us (2%)
    pallas_call x1, Pallas kernels, body(): pl.pallas_call(functools.partial(attention_kernel, n, tp, heads), out_sha...  108 us
    dot_general x1, matrix products, body(): jnp.dot(normed_in, w_key, preferred_element_type=jnp.float32)  3.46 us

profile of v1, /device:TPU:13, one launch (start us, length us, event | category | flops | bytes accessed | tf_op | source)
XLA Modules:
  0.0 128.5 jit_solution(11392069008401908750)
XLA Ops:
  1.9 0.7 dynamic_slice.3
  2.7 1.6 %fusion = f32[129]{0:T(256)S(1)} fusion(bf16[1,4096]{1,0:T(2,128)(2,1)} %param.16, bf16[128,4096]{1,0:T(8,128)(2,1)} %param.15), kind=kLoop, calls=%fused_computation.2 | loop fusion | flops 3170175 | bytes 1057284 | tf_op jit(solution)/shard_map/reduce_sum | solution.py:18
  4.3 0.7 broadcast_in_dim.59.off_ref
  4.9 1.3 %broadcast_in_dim.63.gain_ref = bf16[1,2048]{1,0:T(2,128)(2,1)} reshape(bf16[2048]{0:T(1024)(128)(2,1)} %param.28) | data formatting | bytes 8192 | tf_op jit(solution)/shard_map/broadcast_in_dim | solution.py:273
  6.2 0.7 convert_element_type.24
  6.9 0.7 broadcast_select_fusion.dbias_ref
  7.6 0.7 broadcast_select_fusion.1.cbias_ref
  8.3 0.0 copy-start.1
  8.3 0.0 copy-start.2
  8.3 0.0 copy-start.3
  8.3 3.5 %convolution_convert_fusion.2 = bf16[129,512]{1,0:T(8,128)(2,1)S(1)} fusion(bf16[4096,512]{1,0:T(8,128)(2,1)} %param.19, f32[4096]{0:T(1024)S(1)} %convert_element_type.24, f32[129]{0:T(256)S(1)} %add_rsqrt_fusion, bf16[1,4096]{1,0:T(2,128)(2,1)} %param.16, bf16[128,4096]{1,0:T(8,128)(2,1)} %param.15), kind=kOutput, calls=%fused_computation.7 | convolution fusion | flops 544829952 | bytes 5400068 | tf_op jit(solution)/shard_map/dot_general | solution.py:235
  11.7 0.6 slice.40
  12.3 0.7 slice.35.k_ref
  13.0 0.0 copy-done.1
  13.0 0.0 copy-done.2
  13.0 0.0 copy-done.3
  13.0 0.0 copy-start.4
  13.0 0.8 convolution_convert_fusion.1
  13.8 0.6 slice.41
  14.4 0.7 slice.36.v_ref
  15.1 0.1 copy-done.4
  15.2 0.8 convolution_convert_fusion.3
  16.0 0.6 slice.37.dq_ref
  16.6 0.7 slice.34.q_ref
  17.2 0.0 copy-start
  17.2 108.1 %attend.1 = bf16[144,2048]{1,0:T(8,128)(2,1)} custom-call(bf16[128,512]{1,0:T(8,128)(2,1)} %slice.34.q_ref, bf16[128,512]{1,0:T(8,128)(2,1)} %slice.35.k_ref, bf16[128,512]{1,0:T(8,128)(2,1)} %slice.36.v_ref, bf16[1,512]{1,0:T(2,128)(2,1)} %slice.37.dq_ref, bf16[1024,512]{1,0:T(8,128)(2,1)} %ck_ref.1, bf16[1024,512]{1,0:T(8,128)(2,1)} %cv_ref.1, ...), custom_call_target="tpu_custom_call" | custom-call | tf_op jit(solution)/shard_map/attend/pallas_call | solution.py:252
  125.3 0.0 copy-done
  125.3 1.8 %convolution_convert_fusion = bf16[144,1024]{1,0:T(8,128)(2,1)S(1)} fusion(bf16[144,2048]{1,0:T(8,128)(2,1)} %attend.1, bf16[2048,1024]{1,0:T(8,128)(2,1)S(1)} %copy-done), kind=kOutput, calls=%fused_computation.5 | convolution fusion | flops 604127232 | bytes 5079040 | tf_op jit(solution)/shard_map/dot_general | solution.py:275
  127.2 0.6 slice.39
  127.8 0.7 slice.38
  (4 shorter events, 0.0 us)
Async XLA Ops:
  8.3 4.7 %copy-start.1 = (bf16[128,4096]{1,0:T(8,128)(2,1)S(1)}, bf16[128,4096]{1,0:T(8,128)(2,1)}, u32[]{:S(2)}) copy-start(bf16[128,4096]{1,0:T(8,128)(2,1)} %param.15) | copy-start | bytes 3145732
  8.3 4.7 %copy-start.2 = (bf16[1,4096]{1,0:T(2,128)(2,1)S(1)}, bf16[1,4096]{1,0:T(2,128)(2,1)}, u32[]{:S(2)}) copy-start(bf16[1,4096]{1,0:T(2,128)(2,1)} %param.16) | copy-start | bytes 24580
  8.3 4.7 %copy-start.3 = (bf16[4096,512]{1,0:T(8,128)(2,1)S(1)}, bf16[4096,512]{1,0:T(8,128)(2,1)}, u32[]{:S(2)}) copy-start(bf16[4096,512]{1,0:T(8,128)(2,1)} %param.20) | copy-start | bytes 12582916
  13.0 2.2 %copy-start.4 = (bf16[4096,512]{1,0:T(8,128)(2,1)S(1)}, bf16[4096,512]{1,0:T(8,128)(2,1)}, u32[]{:S(2)}) copy-start(bf16[4096,512]{1,0:T(8,128)(2,1)} %param.18) | copy-start | bytes 12582916
  17.2 108.1 %copy-start = (bf16[2048,1024]{1,0:T(8,128)(2,1)S(1)}, bf16[2048,1024]{1,0:T(8,128)(2,1)}, u32[]{:S(2)}) copy-start(bf16[2048,1024]{1,0:T(8,128)(2,1)} %param.29) | copy-start | bytes 12582916

commit v2 on v1

--- a/solution.py
+++ b/solution.py
@@ -56,8 +56,8 @@
 
 def attention_kernel(
     n, tp, heads, q_ref, k_ref, v_ref, dq_ref, ck_ref, cv_ref, cbias_ref, off_ref, dk_ref, dv_ref,
-    dbias_ref, gain_ref, out_ref, qg, kg, vg, osend, orecv, tsend, trecv, acc, later_s, att, attg,
-    q_ss, q_rs, k_ss, k_rs, v_ss, v_rs, o_ss, o_rs, t_ss, t_rs, a_ss, a_rs,
+    dbias_ref, gain_ref, out_ref, qg, osend, orecv, psend, precv, tsend, trecv, ptot, later_s, att, attg,
+    q_ss, q_rs, p_ss, p_rs, o_ss, o_rs, t_ss, t_rs, a_ss, a_rs,
 ):
     me = lax.axis_index("kv")
     mine = lax.axis_index("tp")
@@ -86,11 +86,7 @@
             remote(src, dst.at[me], ss.at[s], rs.at[me], peer).start()
 
     send_all(q_ref, qg, q_ss, q_rs)
-    send_all(k_ref, kg, k_ss, k_rs)
-    send_all(v_ref, vg, v_ss, v_rs)
     qg[me] = q_ref[...]
-    kg[me] = k_ref[...]
-    vg[me] = v_ref[...]
 
     wide = suffix_matrix(chunk)
     width = heads * HEAD
@@ -114,6 +110,15 @@
     att[pl.ds(rows, 16), :] = dec_rows.astype(att.dtype)
 
     lane = lax.broadcasted_iota(jnp.int32, (rows, 128), 1)
+    narrow = suffix_matrix(rows)
+    qrow = lax.broadcasted_iota(jnp.int32, (rows, rows), 0)
+    kcol = lax.broadcasted_iota(jnp.int32, (rows, rows), 1)
+    for c in range(n):
+
+        @pl.when(c > me)
+        def _():
+            precv[c] = jnp.zeros((rows, width), jnp.bfloat16)
+
 
     def block(s, carry):
         owner = lax.rem(me + s, n)
@@ -134,7 +139,23 @@
             )
             osend[owner, :, cols] = out.astype(jnp.bfloat16)
             totals = jnp.where(lane == h, total, totals)
-        tsend[owner] = jnp.transpose(totals)[0:8, :]
+        ptot[...] = totals
+
+        @pl.when(owner >= me)
+        def _():
+            seen = (me * rows + kcol) < (owner * rows + qrow)
+            totals = ptot[...]
+            for h in range(heads):
+                cols = pl.ds(h * HEAD, HEAD)
+                z = dot_t(qg[owner, :, cols], k_ref[:, cols]) * scale + off_ref[h : h + 1, 0:1]
+                z = jnp.where(seen, z, HIDDEN)
+                inner = suffix_keep(z, narrow)
+                weight = jnp.exp(z + inner).astype(jnp.bfloat16)
+                psend[owner, :, cols] = dot(weight, v_ref[:, cols]).astype(jnp.bfloat16)
+                totals = jnp.where(lane == heads + h, inner[:, 0:1], totals)
+            ptot[...] = totals
+
+        tsend[owner] = jnp.transpose(ptot[...])[0:8, :]
 
         @pl.when(s > 0)
         def _():
@@ -142,63 +163,56 @@
             remote(tsend.at[owner], trecv.at[place], t_ss.at[s], t_rs.at[me], owner).start()
             remote(osend.at[owner], orecv.at[me], o_ss.at[s], o_rs.at[me], owner).start()
 
+        @pl.when(owner > me)
+        def _():
+            remote(psend.at[owner], precv.at[me], p_ss.at[s], p_rs.at[me], owner).start()
+
         return carry
 
     lax.fori_loop(0, n, block, 0)
     orecv[me] = osend[me]
+    precv[me] = psend[me]
     trecv[pl.ds(pl.multiple_of(me * 8, 8), 8), :] = tsend[me]
-
-    for s in range(1, n):
-        peer = lax.rem(me + s, n)
-        remote(k_ref, kg.at[peer], k_ss.at[s], k_rs.at[peer], peer).wait()
-        remote(v_ref, vg.at[peer], v_ss.at[s], v_rs.at[peer], peer).wait()
-        remote(q_ref, qg.at[peer], q_ss.at[s], q_rs.at[peer], peer).wait_send()
-
-    narrow = suffix_matrix(rows)
-    qrow = lax.broadcasted_iota(jnp.int32, (rows, rows), 0)
-    kcol = lax.broadcasted_iota(jnp.int32, (rows, rows), 1)
-    acc[...] = jnp.zeros_like(acc)
-
-    def piece(step, later):
-        j = n - 1 - step
-        seen = (j * rows + kcol) < (me * rows + qrow)
-        nexts = []
-        for h in range(heads):
-            cols = pl.ds(h * HEAD, HEAD)
-            z = dot_t(q_ref[:, cols], kg[j, :, cols]) * scale + off_ref[h : h + 1, 0:1]
-            z = jnp.where(seen, z, HIDDEN)
-            inner = suffix_keep(z, narrow)
-            weight = jnp.exp(z + inner).astype(jnp.bfloat16)
-            acc[:, cols] += dot(weight, vg[j, :, cols]) * jnp.exp(later[h])
-            nexts.append(later[h] + inner[:, 0:1])
-        return tuple(nexts)
-
-    piece_total = lax.fori_loop(
-        0, n, piece, tuple(jnp.zeros((rows, 1), jnp.float32) for _ in range(heads))
-    )
 
     for s in range(1, n):
         peer = lax.rem(me + s, n)
         place = pl.ds(pl.multiple_of(peer * 8, 8), 8)
         remote(tsend.at[peer], trecv.at[place], t_ss.at[s], t_rs.at[peer], peer).wait()
         remote(osend.at[peer], orecv.at[peer], o_ss.at[s], o_rs.at[peer], peer).wait()
+        remote(q_ref, qg.at[peer], q_ss.at[s], q_rs.at[peer], peer).wait_send()
+        pieces = remote(psend.at[peer], precv.at[peer], p_ss.at[s], p_rs.at[peer], peer)
+
+        @pl.when(peer > me)
+        def _():
+            pieces.wait_send()
+
+        @pl.when(peer < me)
+        def _():
+            pieces.wait_recv()
 
     run = jnp.zeros((8, 128), jnp.float32)
     later_s[...] = jnp.zeros_like(later_s)
     for c in reversed(range(n)):
         later_s[c * 8 : c * 8 + 8, :] = run
         run = run + trecv[c * 8 : c * 8 + 8, :]
+    later_s[n * 8 : n * 8 + 8, :] = run
     factors = [
         jnp.exp(jnp.transpose(later_s[g * 128 : g * 128 + 128, :]))
         for g in range(later_s.shape[0] // 128)
     ]
+
+    def factor(c, row):
+        group, spot = divmod(c * 8 + row, 128)
+        return factors[group][:, spot : spot + 1]
+
     for h in range(heads):
         cols = pl.ds(h * HEAD, HEAD)
         mixed = jnp.zeros((rows, HEAD), jnp.float32)
+        pieces = jnp.zeros((rows, HEAD), jnp.float32)
         for c in range(n):
-            group, spot = divmod(c * 8 + h, 128)
-            mixed += orecv[c, :, cols].astype(jnp.float32) * factors[group][:, spot : spot + 1]
-        mixed = mixed * jnp.exp(piece_total[h]) + acc[:, cols]
+            mixed += orecv[c, :, cols].astype(jnp.float32) * factor(c, h)
+            pieces += precv[c, :, cols].astype(jnp.float32) * factor(c, heads + h)
+        mixed = mixed * factor(n, heads + h) + pieces
         att[pl.ds(0, rows), cols] = mixed.astype(att.dtype)
 
     for s in range(1, tp):
@@ -245,7 +259,7 @@
         spots < decoding_cache_length[:, None, None], offset[None, :, None], HIDDEN
     )
     wide_offset = jnp.broadcast_to(offset[:, None], (8, 128))
-    trows = -(-n * 8 // 128) * 128
+    trows = -(-(n + 1) * 8 // 128) * 128
     vmem = pl.BlockSpec(memory_space=pltpu.VMEM)
     dma = pltpu.SemaphoreType.DMA
     block = pltpu.VMEM((n, rows, width), jnp.bfloat16)
@@ -258,11 +272,11 @@
             block, block, block, block, block,
             pltpu.VMEM((n, 8, 128), jnp.float32),
             pltpu.VMEM((trows, 128), jnp.float32),
-            pltpu.VMEM((rows, width), jnp.float32),
+            pltpu.VMEM((rows, 128), jnp.float32),
             pltpu.VMEM((trows, 128), jnp.float32),
             pltpu.VMEM((rows + 16, width), jnp.bfloat16),
             pltpu.VMEM((tp, rows + 16, width), jnp.bfloat16),
-        ] + [dma((n,)) for _ in range(10)] + [dma((tp,)), dma((tp,))],
+        ] + [dma((n,)) for _ in range(8)] + [dma((tp,)), dma((tp,))],
         compiler_params=pltpu.CompilerParams(
             collective_id=0, has_side_effects=True, vmem_limit_bytes=56 * 1024 * 1024
         ),

time: 129 us -> 106 us (0.82)
  Pallas kernels: 108 us -> 84.4 us
    pallas_call x1, Pallas kernels: 108 us -> 84.4 us  [body(): pl.pallas_call(functools.partial(attention_kernel, n, tp, heads), out_sha...]
where the time goes in v2:
time: 106 us; the launch traced here: 105 us
  Pallas kernels  84.4 us (80%)
  local copies, waits for them, and re-layouts  7.92 us (7%)
  matrix products  6.87 us (6%)
  other arithmetic  3.63 us (3%)
  between operations  2 us (2%)
    pallas_call x1, Pallas kernels, body(): pl.pallas_call(functools.partial(attention_kernel, n, tp, heads), out_sha...  84.4 us
    dot_general x1, matrix products, body(): jnp.dot(normed_in, w_key, preferred_element_type=jnp.float32)  3.46 us

profile of v2, /device:TPU:13, one launch (start us, length us, event | category | flops | bytes accessed | tf_op | source)
XLA Modules:
  0.0 104.9 jit_solution(18211609830521121482)
XLA Ops:
  1.9 0.7 dynamic_slice.3
  2.7 1.6 %fusion = f32[129]{0:T(256)S(1)} fusion(bf16[1,4096]{1,0:T(2,128)(2,1)} %param.16, bf16[128,4096]{1,0:T(8,128)(2,1)} %param.15), kind=kLoop, calls=%fused_computation.2 | loop fusion | flops 3170175 | bytes 1057284 | tf_op jit(solution)/shard_map/reduce_sum | solution.py:18
  4.3 0.7 broadcast_in_dim.59.off_ref
  4.9 1.3 %broadcast_in_dim.63.gain_ref = bf16[1,2048]{1,0:T(2,128)(2,1)} reshape(bf16[2048]{0:T(1024)(128)(2,1)} %param.28) | data formatting | bytes 8192 | tf_op jit(solution)/shard_map/broadcast_in_dim | solution.py:287
  6.2 0.7 convert_element_type.24
  6.9 0.7 broadcast_select_fusion.dbias_ref
  7.6 0.7 broadcast_select_fusion.1.cbias_ref
  8.3 0.0 copy-start.1
  8.3 0.0 copy-start.2
  8.3 0.0 copy-start.3
  8.3 3.5 %convolution_convert_fusion.2 = bf16[129,512]{1,0:T(8,128)(2,1)S(1)} fusion(bf16[4096,512]{1,0:T(8,128)(2,1)} %param.19, f32[4096]{0:T(1024)S(1)} %convert_element_type.24, f32[129]{0:T(256)S(1)} %add_rsqrt_fusion, bf16[1,4096]{1,0:T(2,128)(2,1)} %param.16, bf16[128,4096]{1,0:T(8,128)(2,1)} %param.15), kind=kOutput, calls=%fused_computation.7 | convolution fusion | flops 544829952 | bytes 5400068 | tf_op jit(solution)/shard_map/dot_general | solution.py:249
  11.7 0.6 slice.40
  12.3 0.7 slice.35.k_ref
  13.0 0.0 copy-done.1
  13.0 0.0 copy-done.2
  13.0 0.0 copy-done.3
  13.0 0.0 copy-start.4
  13.0 0.8 convolution_convert_fusion.1
  13.8 0.6 slice.41
  14.4 0.7 slice.36.v_ref
  15.1 0.1 copy-done.4
  15.2 0.8 convolution_convert_fusion.3
  16.0 0.6 slice.37.dq_ref
  16.6 0.7 slice.34.q_ref
  17.2 0.0 copy-start
  17.2 84.4 %attend.1 = bf16[144,2048]{1,0:T(8,128)(2,1)} custom-call(bf16[128,512]{1,0:T(8,128)(2,1)} %slice.34.q_ref, bf16[128,512]{1,0:T(8,128)(2,1)} %slice.35.k_ref, bf16[128,512]{1,0:T(8,128)(2,1)} %slice.36.v_ref, bf16[1,512]{1,0:T(2,128)(2,1)} %slice.37.dq_ref, bf16[1024,512]{1,0:T(8,128)(2,1)} %ck_ref.1, bf16[1024,512]{1,0:T(8,128)(2,1)} %cv_ref.1, ...), custom_call_target="tpu_custom_call" | custom-call | tf_op jit(solution)/shard_map/attend/pallas_call | solution.py:266
  101.7 0.0 copy-done
  101.7 1.8 %convolution_convert_fusion = bf16[144,1024]{1,0:T(8,128)(2,1)S(1)} fusion(bf16[144,2048]{1,0:T(8,128)(2,1)} %attend.1, bf16[2048,1024]{1,0:T(8,128)(2,1)S(1)} %copy-done), kind=kOutput, calls=%fused_computation.5 | convolution fusion | flops 604127232 | bytes 5079040 | tf_op jit(solution)/shard_map/dot_general | solution.py:289
  103.6 0.6 slice.39
  104.2 0.7 slice.38
  (4 shorter events, 0.0 us)
Async XLA Ops:
  8.3 4.7 %copy-start.1 = (bf16[128,4096]{1,0:T(8,128)(2,1)S(1)}, bf16[128,4096]{1,0:T(8,128)(2,1)}, u32[]{:S(2)}) copy-start(bf16[128,4096]{1,0:T(8,128)(2,1)} %param.15) | copy-start | bytes 3145732
  8.3 4.7 %copy-start.2 = (bf16[1,4096]{1,0:T(2,128)(2,1)S(1)}, bf16[1,4096]{1,0:T(2,128)(2,1)}, u32[]{:S(2)}) copy-start(bf16[1,4096]{1,0:T(2,128)(2,1)} %param.16) | copy-start | bytes 24580
  8.3 4.7 %copy-start.3 = (bf16[4096,512]{1,0:T(8,128)(2,1)S(1)}, bf16[4096,512]{1,0:T(8,128)(2,1)}, u32[]{:S(2)}) copy-start(bf16[4096,512]{1,0:T(8,128)(2,1)} %param.20) | copy-start | bytes 12582916
  13.0 2.2 %copy-start.4 = (bf16[4096,512]{1,0:T(8,128)(2,1)S(1)}, bf16[4096,512]{1,0:T(8,128)(2,1)}, u32[]{:S(2)}) copy-start(bf16[4096,512]{1,0:T(8,128)(2,1)} %param.18) | copy-start | bytes 12582916
  17.2 84.5 %copy-start = (bf16[2048,1024]{1,0:T(8,128)(2,1)S(1)}, bf16[2048,1024]{1,0:T(8,128)(2,1)}, u32[]{:S(2)}) copy-start(bf16[2048,1024]{1,0:T(8,128)(2,1)} %param.29) | copy-start | bytes 12582916
